TPU v7x, 32 devices: a whole 2x2x4 slice. The times are simulated.
32 devices in a mesh: sp: 8 (over z, x), tp: 4 (over y, core).
Axes of the slice: x: 2, y: 2, z: 4, core: 2. Of those that a mesh axis runs over, the one named last changes fastest.
Arguments:
- hidden_in: bfloat16 [512, 2048], P(('sp', 'tp')), may hold values from -6 to 6
- pre_gain: float32 [2048], replicated, may hold values from 0.5 to 1.5
- w_query: bfloat16 [2048, 1024], P(None, 'tp'), may hold values from -0.4375 to 0.4375
- w_key: bfloat16 [2048, 1024], P(None, 'tp'), may hold values from -0.125 to 0.125
- w_value: bfloat16 [2048, 1024], P(None, 'tp'), may hold values from -0.125 to 0.125
- stick_offset: float32 [8], P('tp'), may hold values from -15.2 to -14.2
- w_glu_a: bfloat16 [2048, 1024], P(None, 'tp'), may hold values from -0.125 to 0.125
- w_glu_b: bfloat16 [2048, 1024], P(None, 'tp'), may hold values from -0.125 to 0.125
- w_gate_attn: bfloat16 [2048, 2048], P(None, 'tp'), may hold values from -0.125 to 0.125
- w_gate_conv: bfloat16 [2048, 2048], P(None, 'tp'), may hold values from -0.125 to 0.125
- conv_taps: float32 [31, 1024], P(None, 'tp'), may hold values from -1 to 1
- conv_bias: float32 [1024], P('tp'), may hold values from -0.6 to 0.6
- norm_gain: float32 [1024], P('tp'), may hold values from 0.5 to 1.5
- norm_shift: float32 [1024], P('tp'), may hold values from -0.6 to 0.6
- w_attn_out: bfloat16 [1024, 2048], P('tp'), may hold values from -0.4375 to 0.4375
- w_conv_out: bfloat16 [1024, 2048], P('tp'), may hold values from -0.1875 to 0.1875
- post_gain: float32 [2048], P('tp'), may hold values from 0.5 to 1.5
Outputs:
- mixed: bfloat16 [512, 2048], P('sp', 'tp')
All inputs are finite; a program needn't handle non-finite values.
Results may differ from a plain program's by a relative error of at most 0.015.
Values may be sent and summed in bfloat16 or wider, within the bound.
A program may use at most 64 MiB of HBM per device.

v0:
```python
from functools import partial
import math

import jax
import jax.numpy as jnp
from jax import lax
from jax.sharding import PartitionSpec as P

D = 2048
HEAD_DIM = 128
CONV_CH = 1024
WIDTH = 31


epsilon = 1e-06


def shortened(x):
    def short(part):
        return part.astype(jnp.bfloat16) if part.dtype == jnp.float32 else part

    return jax.tree.map(short, x)


def passed_along(value, axis, steps):
    count = lax.axis_size(axis)
    initial, last = max(0, -steps), min(count, count - steps)
    return lax.ppermute(value, axis, [(source, source + steps) for source in range(initial, last)])


def summed_rows(product, extent, axis):
    everything = product(jnp.int32(0), lax.axis_size(axis) * extent)
    own = lax.psum_scatter(everything.astype(jnp.bfloat16), axis, scatter_dimension=0, tiled=True)
    return own.astype(jnp.float32)


def stick_terms(query_heads, key_block, offsets, causal):
    scores = jnp.einsum("thd,shd->hts", query_heads, key_block, preferred_element_type=jnp.float32)
    scores = scores / math.sqrt(HEAD_DIM) + offsets[:, None, None]
    log_rest = jnp.where(causal[None], jax.nn.log_sigmoid(-scores), 0.0)
    inside = lax.cumsum(log_rest, axis=2, reverse=True) - log_rest
    return (scores, log_rest, inside)


def weighted_values(scores, inside, outside, causal, value_block):
    weights = jnp.where(causal[None], jnp.exp(jax.nn.log_sigmoid(scores) + inside + outside), 0.0)
    return jnp.einsum(
        "hts,shd->thd", weights, value_block.astype(jnp.float32), precision=lax.Precision.HIGHEST
    )


def term_for(matrix, activations, offset, length):
    columns = lax.dynamic_slice_in_dim(matrix, offset, length, 1)
    return lax.dot_general(
        columns, activations, (((0,), (1,)), ((), ())), preferred_element_type=jnp.float32
    )


def held_bf16(values):
    return lax.optimization_barrier(values.astype(jnp.bfloat16))


def shards(
    hidden_in,
    pre_gain,
    w_query,
    w_key,
    w_value,
    stick_offset,
    w_glu_a,
    w_glu_b,
    w_gate_attn,
    w_gate_conv,
    conv_taps,
    conv_bias,
    norm_gain,
    norm_shift,
    w_attn_out,
    w_conv_out,
    post_gain,
):
    weight_list = (w_query, w_key, w_value, w_glu_a, w_glu_b, w_gate_attn, w_gate_conv)

    def project(portion):
        values = portion.astype(jnp.float32)
        inverse = lax.rsqrt(jnp.mean(values * values, axis=1, keepdims=True) + epsilon)
        normed = (values * inverse * pre_gain).astype(jnp.bfloat16)
        return jnp.concatenate(
            [
                jnp.dot(normed, weight, preferred_element_type=jnp.float32).astype(jnp.bfloat16)
                for weight in weight_list
            ],
            axis=1,
        )

    joined = lax.optimization_barrier(project(lax.all_gather(hidden_in, "tp", axis=0, tiled=True)))
    pieces_list = []
    cursor = 0
    for weight in weight_list:
        pieces_list.append(joined[:, cursor : cursor + weight.shape[1]])
        cursor = cursor + weight.shape[1]
    queries, key_rows, value_rows, glu_left, glu_right, gate_attn, gate_conv = pieces_list
    row_count = joined.shape[0]
    head_count = stick_offset.shape[0]
    kv_width = key_rows.shape[1]
    my_index = lax.axis_index("sp")
    local_iota = jnp.arange(row_count, dtype=jnp.int32)
    query_pos = my_index * row_count + local_iota
    query_heads = queries.reshape(row_count, head_count, HEAD_DIM)

    def chain_step(log_total, summed, incoming, block_index):
        key_block = incoming[:, :kv_width].reshape(row_count, head_count, HEAD_DIM)
        value_block = incoming[:, kv_width:].reshape(row_count, head_count, HEAD_DIM)
        key_pos = block_index * row_count + local_iota
        causal = (key_pos[None, :] < query_pos[:, None]) & (block_index >= 0)
        scores, log_rest, inside = stick_terms(query_heads, key_block, stick_offset, causal)
        summed = summed + weighted_values(
            scores, inside, log_total[:, :, None], causal, value_block
        )
        return (log_total + jnp.sum(log_rest, axis=2), summed)

    travelling = jnp.concatenate([key_rows, value_rows], axis=1)
    log_total, summed = chain_step(
        jnp.zeros((head_count, row_count), jnp.float32),
        jnp.zeros((row_count, head_count, HEAD_DIM), jnp.float32),
        travelling,
        my_index,
    )

    def advance(rounds, loop_state):
        moving, log_sofar, summed_sofar = loop_state
        moving = passed_along(shortened(moving), "sp", 1).astype(moving.dtype)
        log_sofar, summed_sofar = chain_step(log_sofar, summed_sofar, moving, my_index - rounds)
        return (moving, log_sofar, summed_sofar)

    loop_state = lax.fori_loop(1, lax.axis_size("sp"), advance, (travelling, log_total, summed))
    summed = loop_state[2]
    attended = summed.reshape(row_count, head_count * HEAD_DIM).astype(jnp.bfloat16)
    gated_in = held_bf16(
        glu_left.astype(jnp.float32) * jax.nn.sigmoid(glu_right.astype(jnp.float32))
    )
    before = passed_along(gated_in[row_count - (WIDTH - 1) :], "sp", 1)
    padded = jnp.concatenate([before, gated_in], axis=0).astype(jnp.float32)
    channels = gated_in.shape[1]
    convolved = (
        lax.conv_general_dilated(
            padded[None],
            conv_taps.reshape(WIDTH, 1, channels),
            (1,),
            "VALID",
            dimension_numbers=("NWC", "WIO", "NWC"),
            feature_group_count=channels,
            precision=lax.Precision.HIGHEST,
        )[0]
        + conv_bias
    )
    first_sum, second_sum = lax.psum(
        (jnp.sum(convolved, axis=1), jnp.sum(convolved * convolved, axis=1)), "tp"
    )
    mean_row = first_sum / CONV_CH
    centered = convolved - mean_row[:, None]
    spread = second_sum / CONV_CH - mean_row * mean_row
    conv_normed = jax.nn.silu(
        centered * lax.rsqrt(spread + epsilon)[:, None] * norm_gain + norm_shift
    ).astype(jnp.bfloat16)
    out_cols = post_gain.shape[0]
    attn_sum = summed_rows(partial(term_for, w_attn_out, attended), out_cols, "tp")
    conv_sum = summed_rows(partial(term_for, w_conv_out, conv_normed), out_cols, "tp")
    attn_branch = held_bf16(jnp.transpose(attn_sum)).astype(jnp.float32)
    conv_branch = held_bf16(jnp.transpose(conv_sum)).astype(jnp.float32)
    merged = (
        jax.nn.sigmoid(gate_attn.astype(jnp.float32)) * attn_branch
        + jax.nn.sigmoid(gate_conv.astype(jnp.float32)) * conv_branch
    )
    squares = lax.psum(jnp.sum(merged * merged, axis=1), "tp")
    return (merged * lax.rsqrt(squares / D + epsilon)[:, None] * post_gain).astype(jnp.bfloat16)


def solution(mesh):
    in_specs = (
        P(("sp", "tp"), None),
        P(),
        P(None, "tp"),
        P(None, "tp"),
        P(None, "tp"),
        P("tp"),
        P(None, "tp"),
        P(None, "tp"),
        P(None, "tp"),
        P(None, "tp"),
        P(None, "tp"),
        P("tp"),
        P("tp"),
        P("tp"),
        P("tp", None),
        P("tp", None),
        P("tp"),
    )
    out_specs = P("sp", "tp")
    return jax.shard_map(shards, mesh=mesh, in_specs=in_specs, out_specs=out_specs, check_vma=False)
```

profile of v0, /device:TPU:19, one launch (start us, length us, event | category | flops | bytes accessed | tf_op | source)
XLA Modules:
  0.0 155.5 jit_solution(35718758757625549)
XLA Ops:
  6.5 6.6 %all_gather.3 = bf16[64,2048]{1,0:T(8,128)(2,1)S(1)} all-gather(bf16[16,2048]{1,0:T(8,128)(2,1)} %param.19), channel_id=1, replica_groups=mesh['sp'=8,'tp'=4] {'tp'}, dimensions={0}, use_global_device_ids=true | all-gather | bytes 327680 | tf_op jit(solution)/shard_map/all_gather | solution.py:96
  13.3 1.7 %fusion.39 = bf16[64,2304]{1,0:T(8,128)(2,1)S(1)} fusion(bf16[2048,256]{1,0:T(8,128)(2,1)} %param.21, bf16[64,2048]{1,0:T(8,128)(2,1)S(1)} %all_gather.3, f32[2048]{0:T(1024)} %param.20, f32[64]{0:T(128)S(1)} %add_rsqrt_fusion.2), kind=kOutput, calls=%fused_computation.58 | convolution fusion | flops 67649536 | bytes 1351936 | tf_op jit(solution)/shard_map/dot_general | solution.py:90
  19.6 3.2 %collective-permute-start.1 = (bf16[30,256]{1,0:T(8,128)(2,1)S(1)}, bf16[30,256]{1,0:T(8,128)(2,1)}, u32[]{:S(2)}, u32[]{:S(2)}) collective-permute-start(bf16[30,256]{1,0:T(8,128)(2,1)S(1)} %slice.58), channel_id=1, source_target_pairs={{0,4},{4,8},{8,12},{12,16},{16,20},{20,24},{24,28},{1,5},{5,9},{9,... | collective-permute-start | bytes 46088 | tf_op jit(solution)/shard_map/ppermute | solution.py:28
  25.3 62.0 %while.18 = (s32[]{:T(128)}, bf16[64,512]{1,0:T(8,128)(2,1)S(1)}, f32[2,64]{1,0:T(2,128)S(1)}, f32[64,2,128]{2,0,1:T(8,128)}, s32[]{:T(128)}, /*index=5*/bf16[64...) while((s32[]{:T(128)}, bf16[64,512]{1,0:T(8,128)(2,1)S(1)}, ...), condition=%wide.region_6.7_spmd.clone, body=%wide.region_3.6_spmd.clone.sunk | while | flops 15560837 | bytes 1142483 | solution.py:136
  25.3 3.2 %collective-permute-start = (bf16[64,512]{1,0:T(8,128)(2,1)S(1)}, bf16[64,512]{1,0:T(8,128)(2,1)S(1)}, u32[]{:S(2)}, u32[]{:S(2)}) collective-permute-start(bf16[64,512]{1,0:T(8,128)(2,1)S(1)} %get-tuple-element.307), channel_id=1, source_target_pairs={{0,4},{4,8},{8,12},{12,16},{16,20},{20,24},{24,28},{1,5},{5,9},{9,... | collective-permute-start | bytes 196616 | tf_op jit(solution)/shard_map/while/body/eval_jaxpr/ppermute | solution.py:28
  28.6 1.8 %collective-permute-done = bf16[64,512]{1,0:T(8,128)(2,1)S(1)} collective-permute-done((bf16[64,512]{1,0:T(8,128)(2,1)S(1)}, bf16[64,512]{1,0:T(8,128)(2,1)S(1)}, u32[]{:S(2)}, u32[]{:S(2)}) %collective-permute-start) | collective-permute-done | bytes 65568 | tf_op jit(solution)/shard_map/while/body/eval_jaxpr/ppermute | solution.py:28
  31.7 1.8 %fusion.104 = f32[64,2,128]{2,0,1:T(8,128)} fusion(f32[64,2,128]{2,0,1:T(8,128)} %get-tuple-element.309, f32[2,64,64]{1,2,0:T(8,128)S(1)} %copy.102, f32[2,64,64]{1,2,0:T(8,128)S(1)} %get-tuple-element.289, bf16[8,2,8,128]{3,2,1,0:T(8,128)(2,1)S(1)} %get-tuple-element.293, f32[2,64]{1,0:T(2,128)S(1)} %get-tuple-element.308, ...), kind=kOutput, calls=%fused_computation.3.clone.1 | convolution fusion | flops 12787712 | bytes 238080 | tf_op jit(solution)/shard_map/while/body/eval_jaxpr/hts,shd->thd/dot_general | solution.py:47
  33.5 4.0 %collective-permute-start = (bf16[64,512]{1,0:T(8,128)(2,1)S(1)}, bf16[64,512]{1,0:T(8,128)(2,1)S(1)}, u32[]{:S(2)}, u32[]{:S(2)}) collective-permute-start(bf16[64,512]{1,0:T(8,128)(2,1)S(1)} %get-tuple-element.307), channel_id=1, source_target_pairs={{0,4},{4,8},{8,12},{12,16},{16,20},{20,24},{24,28},{1,5},{5,9},{9,... | collective-permute-start | bytes 196616 | tf_op jit(solution)/shard_map/while/body/eval_jaxpr/ppermute | solution.py:28
  40.2 1.8 %fusion.104 = f32[64,2,128]{2,0,1:T(8,128)} fusion(f32[64,2,128]{2,0,1:T(8,128)} %get-tuple-element.309, f32[2,64,64]{1,2,0:T(8,128)S(1)} %copy.102, f32[2,64,64]{1,2,0:T(8,128)S(1)} %get-tuple-element.289, bf16[8,2,8,128]{3,2,1,0:T(8,128)(2,1)S(1)} %get-tuple-element.293, f32[2,64]{1,0:T(2,128)S(1)} %get-tuple-element.308, ...), kind=kOutput, calls=%fused_computation.3.clone.1 | convolution fusion | flops 12787712 | bytes 238080 | tf_op jit(solution)/shard_map/while/body/eval_jaxpr/hts,shd->thd/dot_general | solution.py:47
  42.0 4.6 %collective-permute-start = (bf16[64,512]{1,0:T(8,128)(2,1)S(1)}, bf16[64,512]{1,0:T(8,128)(2,1)S(1)}, u32[]{:S(2)}, u32[]{:S(2)}) collective-permute-start(bf16[64,512]{1,0:T(8,128)(2,1)S(1)} %get-tuple-element.307), channel_id=1, source_target_pairs={{0,4},{4,8},{8,12},{12,16},{16,20},{20,24},{24,28},{1,5},{5,9},{9,... | collective-permute-start | bytes 196616 | tf_op jit(solution)/shard_map/while/body/eval_jaxpr/ppermute | solution.py:28
  49.2 1.8 %fusion.104 = f32[64,2,128]{2,0,1:T(8,128)} fusion(f32[64,2,128]{2,0,1:T(8,128)} %get-tuple-element.309, f32[2,64,64]{1,2,0:T(8,128)S(1)} %copy.102, f32[2,64,64]{1,2,0:T(8,128)S(1)} %get-tuple-element.289, bf16[8,2,8,128]{3,2,1,0:T(8,128)(2,1)S(1)} %get-tuple-element.293, f32[2,64]{1,0:T(2,128)S(1)} %get-tuple-element.308, ...), kind=kOutput, calls=%fused_computation.3.clone.1 | convolution fusion | flops 12787712 | bytes 238080 | tf_op jit(solution)/shard_map/while/body/eval_jaxpr/hts,shd->thd/dot_general | solution.py:47
  51.1 4.6 %collective-permute-start = (bf16[64,512]{1,0:T(8,128)(2,1)S(1)}, bf16[64,512]{1,0:T(8,128)(2,1)S(1)}, u32[]{:S(2)}, u32[]{:S(2)}) collective-permute-start(bf16[64,512]{1,0:T(8,128)(2,1)S(1)} %get-tuple-element.307), channel_id=1, source_target_pairs={{0,4},{4,8},{8,12},{12,16},{16,20},{20,24},{24,28},{1,5},{5,9},{9,... | collective-permute-start | bytes 196616 | tf_op jit(solution)/shard_map/while/body/eval_jaxpr/ppermute | solution.py:28
  58.3 1.8 %fusion.104 = f32[64,2,128]{2,0,1:T(8,128)} fusion(f32[64,2,128]{2,0,1:T(8,128)} %get-tuple-element.309, f32[2,64,64]{1,2,0:T(8,128)S(1)} %copy.102, f32[2,64,64]{1,2,0:T(8,128)S(1)} %get-tuple-element.289, bf16[8,2,8,128]{3,2,1,0:T(8,128)(2,1)S(1)} %get-tuple-element.293, f32[2,64]{1,0:T(2,128)S(1)} %get-tuple-element.308, ...), kind=kOutput, calls=%fused_computation.3.clone.1 | convolution fusion | flops 12787712 | bytes 238080 | tf_op jit(solution)/shard_map/while/body/eval_jaxpr/hts,shd->thd/dot_general | solution.py:47
  60.1 4.6 %collective-permute-start = (bf16[64,512]{1,0:T(8,128)(2,1)S(1)}, bf16[64,512]{1,0:T(8,128)(2,1)S(1)}, u32[]{:S(2)}, u32[]{:S(2)}) collective-permute-start(bf16[64,512]{1,0:T(8,128)(2,1)S(1)} %get-tuple-element.307), channel_id=1, source_target_pairs={{0,4},{4,8},{8,12},{12,16},{16,20},{20,24},{24,28},{1,5},{5,9},{9,... | collective-permute-start | bytes 196616 | tf_op jit(solution)/shard_map/while/body/eval_jaxpr/ppermute | solution.py:28
  67.3 1.8 %fusion.104 = f32[64,2,128]{2,0,1:T(8,128)} fusion(f32[64,2,128]{2,0,1:T(8,128)} %get-tuple-element.309, f32[2,64,64]{1,2,0:T(8,128)S(1)} %copy.102, f32[2,64,64]{1,2,0:T(8,128)S(1)} %get-tuple-element.289, bf16[8,2,8,128]{3,2,1,0:T(8,128)(2,1)S(1)} %get-tuple-element.293, f32[2,64]{1,0:T(2,128)S(1)} %get-tuple-element.308, ...), kind=kOutput, calls=%fused_computation.3.clone.1 | convolution fusion | flops 12787712 | bytes 238080 | tf_op jit(solution)/shard_map/while/body/eval_jaxpr/hts,shd->thd/dot_general | solution.py:47
  69.2 4.6 %collective-permute-start = (bf16[64,512]{1,0:T(8,128)(2,1)S(1)}, bf16[64,512]{1,0:T(8,128)(2,1)S(1)}, u32[]{:S(2)}, u32[]{:S(2)}) collective-permute-start(bf16[64,512]{1,0:T(8,128)(2,1)S(1)} %get-tuple-element.307), channel_id=1, source_target_pairs={{0,4},{4,8},{8,12},{12,16},{16,20},{20,24},{24,28},{1,5},{5,9},{9,... | collective-permute-start | bytes 196616 | tf_op jit(solution)/shard_map/while/body/eval_jaxpr/ppermute | solution.py:28
  76.4 1.8 %fusion.104 = f32[64,2,128]{2,0,1:T(8,128)} fusion(f32[64,2,128]{2,0,1:T(8,128)} %get-tuple-element.309, f32[2,64,64]{1,2,0:T(8,128)S(1)} %copy.102, f32[2,64,64]{1,2,0:T(8,128)S(1)} %get-tuple-element.289, bf16[8,2,8,128]{3,2,1,0:T(8,128)(2,1)S(1)} %get-tuple-element.293, f32[2,64]{1,0:T(2,128)S(1)} %get-tuple-element.308, ...), kind=kOutput, calls=%fused_computation.3.clone.1 | convolution fusion | flops 12787712 | bytes 238080 | tf_op jit(solution)/shard_map/while/body/eval_jaxpr/hts,shd->thd/dot_general | solution.py:47
  78.2 4.6 %collective-permute-start = (bf16[64,512]{1,0:T(8,128)(2,1)S(1)}, bf16[64,512]{1,0:T(8,128)(2,1)S(1)}, u32[]{:S(2)}, u32[]{:S(2)}) collective-permute-start(bf16[64,512]{1,0:T(8,128)(2,1)S(1)} %get-tuple-element.307), channel_id=1, source_target_pairs={{0,4},{4,8},{8,12},{12,16},{16,20},{20,24},{24,28},{1,5},{5,9},{9,... | collective-permute-start | bytes 196616 | tf_op jit(solution)/shard_map/while/body/eval_jaxpr/ppermute | solution.py:28
  85.4 1.8 %fusion.104 = f32[64,2,128]{2,0,1:T(8,128)} fusion(f32[64,2,128]{2,0,1:T(8,128)} %get-tuple-element.309, f32[2,64,64]{1,2,0:T(8,128)S(1)} %copy.102, f32[2,64,64]{1,2,0:T(8,128)S(1)} %get-tuple-element.289, bf16[8,2,8,128]{3,2,1,0:T(8,128)(2,1)S(1)} %get-tuple-element.293, f32[2,64]{1,0:T(2,128)S(1)} %get-tuple-element.308, ...), kind=kOutput, calls=%fused_computation.3.clone.1 | convolution fusion | flops 12787712 | bytes 238080 | tf_op jit(solution)/shard_map/while/body/eval_jaxpr/hts,shd->thd/dot_general | solution.py:47
  87.3 1.8 %fusion.30 = bf16[2048,64]{0,1:T(8,128)(2,1)} fusion(bf16[256,2048]{1,0:T(8,128)(2,1)S(1)} %copy-done.5, f32[64,2,128]{2,0,1:T(8,128)} %get-tuple-element.159), kind=kOutput, calls=%fused_computation.40 | convolution fusion | flops 67256320 | bytes 1376256 | tf_op jit(solution)/shard_map/dot_general | solution.py:54
  91.2 13.2 %all-reduce = (f32[64]{0:T(128)S(1)}, f32[64]{0:T(128)S(1)}) all-reduce(f32[64]{0:T(128)S(1)} %get-tuple-element.197, f32[64]{0:T(128)S(1)} %get-tuple-element.196), channel_id=1, replica_groups=mesh['sp'=8,'tp'=4] {'tp'}, use_global_device_ids=true, to_apply=%region_11.12 | all-reduce | flops 128 | bytes 1024 | tf_op jit(solution)/shard_map/psum | solution.py:157
  105.5 12.8 %reduce-scatter.3.cloned.1.call-done = bf16[512,64]{0,1:T(8,128)(2,1)} async-done(((bf16[2048,64]{0,1:T(8,128)(2,1)}), bf16[512,64]{0,1:T(8,128)(2,1)}) %reduce-scatter.3.cloned.1.call-update) | async-done | bytes 65552 | tf_op jit(solution)/shard_map/reduce_scatter | solution.py:33
  118.3 22.5 %reduce-scatter.5.cloned.1.call-done = bf16[512,64]{0,1:T(8,128)(2,1)} async-done(((bf16[2048,64]{0,1:T(8,128)(2,1)}), bf16[512,64]{0,1:T(8,128)(2,1)}) %reduce-scatter.5.cloned.1.call-update) | async-done | bytes 65552 | tf_op jit(solution)/shard_map/reduce_scatter | solution.py:33
  141.9 6.0 %psum.23 = f32[64]{0:T(128)S(1)} all-reduce(f32[64]{0:T(128)S(1)} %get-tuple-element.216), channel_id=1, replica_groups=mesh['sp'=8,'tp'=4] {'tp'}, use_global_device_ids=true, to_apply=%region_14.15 | all-reduce | flops 64 | bytes 512 | tf_op jit(solution)/shard_map/psum | solution.py:175
  (145 shorter events, 28.8 us)
Async XLA Ops:
  6.5 11.3 %copy-start = (bf16[2048,512]{1,0:T(8,128)(2,1)S(1)}, bf16[2048,512]{1,0:T(8,128)(2,1)}, u32[]{:S(2)}) copy-start(bf16[2048,512]{1,0:T(8,128)(2,1)} %param.27) | copy-start | bytes 6291460
  6.5 10.2 %copy-start.8 = (f32[2048]{0:T(1024)S(1)}, f32[2048]{0:T(1024)}, u32[]{:S(2)}) copy-start(f32[2048]{0:T(1024)} %param.20) | copy-start | bytes 24580
  6.5 10.2 %copy-start.2 = (bf16[2048,256]{1,0:T(8,128)(2,1)S(1)}, bf16[2048,256]{1,0:T(8,128)(2,1)}, u32[]{:S(2)}) copy-start(bf16[2048,256]{1,0:T(8,128)(2,1)} %param.23) | copy-start | bytes 3145732
  6.5 111.8 %reduce-scatter.3.cloned.1.call-start = ((), (), s32[]{:S(2)}) async-start(), calls=%async_computation.2 | async-start | bytes 327680 | tf_op jit(solution)/shard_map/reduce_scatter | solution.py:33
  13.2 3.9 %copy-start.3 = (bf16[2048,256]{1,0:T(8,128)(2,1)S(1)}, bf16[2048,256]{1,0:T(8,128)(2,1)}, u32[]{:S(2)}) copy-start(bf16[2048,256]{1,0:T(8,128)(2,1)} %param.25) | copy-start | bytes 3145732
  15.0 2.4 %copy-start.4 = (bf16[2048,256]{1,0:T(8,128)(2,1)S(1)}, bf16[2048,256]{1,0:T(8,128)(2,1)}, u32[]{:S(2)}) copy-start(bf16[2048,256]{1,0:T(8,128)(2,1)} %param.26) | copy-start | bytes 3145732
  17.4 1.6 %copy-start.1 = (bf16[2048,512]{1,0:T(8,128)(2,1)S(1)}, bf16[2048,512]{1,0:T(8,128)(2,1)}, u32[]{:S(2)}) copy-start(bf16[2048,512]{1,0:T(8,128)(2,1)} %param.28) | copy-start | bytes 6291460
  17.8 5.1 %copy-start.9 = (f32[2]{0:T(128)S(1)}, f32[2]{0:T(128)}, u32[]{:S(2)}) copy-start(f32[2]{0:T(128)} %param.24) | copy-start | bytes 28
  19.6 3.3 %copy-start.7 = (bf16[64,2304]{1,0:T(8,128)(2,1)}, bf16[64,2304]{1,0:T(8,128)(2,1)S(1)}, u32[]{:S(2)}) copy-start(bf16[64,2304]{1,0:T(8,128)(2,1)S(1)} %fusion.33) | copy-start | bytes 884740
  19.6 69.6 %collective-permute-start.1 = (bf16[30,256]{1,0:T(8,128)(2,1)S(1)}, bf16[30,256]{1,0:T(8,128)(2,1)}, u32[]{:S(2)}, u32[]{:S(2)}) collective-permute-start(bf16[30,256]{1,0:T(8,128)(2,1)S(1)} %slice.58), channel_id=1, source_target_pairs={{0,4},{4,8},{8,12},{12,16},{16,20},{20,24},{24,28},{1,5},{5,9},{9,... | collective-permute-start | bytes 46088 | tf_op jit(solution)/shard_map/ppermute | solution.py:28
  25.3 62.1 %copy-start.5 = (bf16[256,2048]{1,0:T(8,128)(2,1)S(1)}, bf16[256,2048]{1,0:T(8,128)(2,1)}, u32[]{:S(2)}) copy-start(bf16[256,2048]{1,0:T(8,128)(2,1)} %param.33) | copy-start | bytes 3145732
  25.3 5.1 %collective-permute-start = (bf16[64,512]{1,0:T(8,128)(2,1)S(1)}, bf16[64,512]{1,0:T(8,128)(2,1)S(1)}, u32[]{:S(2)}, u32[]{:S(2)}) collective-permute-start(bf16[64,512]{1,0:T(8,128)(2,1)S(1)} %get-tuple-element.307), channel_id=1, source_target_pairs={{0,4},{4,8},{8,12},{12,16},{16,20},{20,24},{24,28},{1,5},{5,9},{9,... | collective-permute-start | bytes 196616 | tf_op jit(solution)/shard_map/while/body/eval_jaxpr/ppermute | solution.py:28
  33.5 5.3 %collective-permute-start = (bf16[64,512]{1,0:T(8,128)(2,1)S(1)}, bf16[64,512]{1,0:T(8,128)(2,1)S(1)}, u32[]{:S(2)}, u32[]{:S(2)}) collective-permute-start(bf16[64,512]{1,0:T(8,128)(2,1)S(1)} %get-tuple-element.307), channel_id=1, source_target_pairs={{0,4},{4,8},{8,12},{12,16},{16,20},{20,24},{24,28},{1,5},{5,9},{9,... | collective-permute-start | bytes 196616 | tf_op jit(solution)/shard_map/while/body/eval_jaxpr/ppermute | solution.py:28
  42.0 5.9 %collective-permute-start = (bf16[64,512]{1,0:T(8,128)(2,1)S(1)}, bf16[64,512]{1,0:T(8,128)(2,1)S(1)}, u32[]{:S(2)}, u32[]{:S(2)}) collective-permute-start(bf16[64,512]{1,0:T(8,128)(2,1)S(1)} %get-tuple-element.307), channel_id=1, source_target_pairs={{0,4},{4,8},{8,12},{12,16},{16,20},{20,24},{24,28},{1,5},{5,9},{9,... | collective-permute-start | bytes 196616 | tf_op jit(solution)/shard_map/while/body/eval_jaxpr/ppermute | solution.py:28
  51.1 5.9 %collective-permute-start = (bf16[64,512]{1,0:T(8,128)(2,1)S(1)}, bf16[64,512]{1,0:T(8,128)(2,1)S(1)}, u32[]{:S(2)}, u32[]{:S(2)}) collective-permute-start(bf16[64,512]{1,0:T(8,128)(2,1)S(1)} %get-tuple-element.307), channel_id=1, source_target_pairs={{0,4},{4,8},{8,12},{12,16},{16,20},{20,24},{24,28},{1,5},{5,9},{9,... | collective-permute-start | bytes 196616 | tf_op jit(solution)/shard_map/while/body/eval_jaxpr/ppermute | solution.py:28
  60.1 5.9 %collective-permute-start = (bf16[64,512]{1,0:T(8,128)(2,1)S(1)}, bf16[64,512]{1,0:T(8,128)(2,1)S(1)}, u32[]{:S(2)}, u32[]{:S(2)}) collective-permute-start(bf16[64,512]{1,0:T(8,128)(2,1)S(1)} %get-tuple-element.307), channel_id=1, source_target_pairs={{0,4},{4,8},{8,12},{12,16},{16,20},{20,24},{24,28},{1,5},{5,9},{9,... | collective-permute-start | bytes 196616 | tf_op jit(solution)/shard_map/while/body/eval_jaxpr/ppermute | solution.py:28
  69.2 5.9 %collective-permute-start = (bf16[64,512]{1,0:T(8,128)(2,1)S(1)}, bf16[64,512]{1,0:T(8,128)(2,1)S(1)}, u32[]{:S(2)}, u32[]{:S(2)}) collective-permute-start(bf16[64,512]{1,0:T(8,128)(2,1)S(1)} %get-tuple-element.307), channel_id=1, source_target_pairs={{0,4},{4,8},{8,12},{12,16},{16,20},{20,24},{24,28},{1,5},{5,9},{9,... | collective-permute-start | bytes 196616 | tf_op jit(solution)/shard_map/while/body/eval_jaxpr/ppermute | solution.py:28
  78.2 5.9 %collective-permute-start = (bf16[64,512]{1,0:T(8,128)(2,1)S(1)}, bf16[64,512]{1,0:T(8,128)(2,1)S(1)}, u32[]{:S(2)}, u32[]{:S(2)}) collective-permute-start(bf16[64,512]{1,0:T(8,128)(2,1)S(1)} %get-tuple-element.307), channel_id=1, source_target_pairs={{0,4},{4,8},{8,12},{12,16},{16,20},{20,24},{24,28},{1,5},{5,9},{9,... | collective-permute-start | bytes 196616 | tf_op jit(solution)/shard_map/while/body/eval_jaxpr/ppermute | solution.py:28
  87.3 3.8 %copy-start.10 = (f32[256]{0:T(256)S(1)}, f32[256]{0:T(256)}, u32[]{:S(2)}) copy-start(f32[256]{0:T(256)} %param.30) | copy-start | bytes 3076
  87.3 17.1 %copy-start.12 = (f32[256]{0:T(256)S(1)}, f32[256]{0:T(256)}, u32[]{:S(2)}) copy-start(f32[256]{0:T(256)} %param.32) | copy-start | bytes 3076
  87.3 17.1 %copy-start.13 = (f32[256]{0:T(256)S(1)}, f32[256]{0:T(256)}, u32[]{:S(2)}) copy-start(f32[256]{0:T(256)} %param.31) | copy-start | bytes 3076
  89.2 15.3 %copy-start.6 = (bf16[256,2048]{1,0:T(8,128)(2,1)S(1)}, bf16[256,2048]{1,0:T(8,128)(2,1)}, u32[]{:S(2)}) copy-start(bf16[256,2048]{1,0:T(8,128)(2,1)} %param.34) | copy-start | bytes 3145732
  89.2 58.8 %copy-start.11 = (f32[512]{0:T(512)S(1)}, f32[512]{0:T(512)}, u32[]{:S(2)}) copy-start(f32[512]{0:T(512)} %param.35) | copy-start | bytes 6148
  89.2 51.6 %reduce-scatter.5.cloned.1.call-start = ((), (), s32[]{:S(2)}) async-start(), calls=%async_computation.3 | async-start | bytes 327680 | tf_op jit(solution)/shard_map/reduce_scatter | solution.py:33
Sparse Core Ops, SparseCore 0:
  89.3 28.9 reduce-scatter.2
  120.8 19.9 reduce-scatter.4
where the time goes:
time: 158 us; the launch traced here: 156 us
  waiting for transfers between devices  44.2 us (28%)
  starting transfers between devices  33.4 us (21%)
  blocking collectives  25.9 us (16%)
  matrix products  24.1 us (15%)
  between operations  13.7 us (9%)
  other arithmetic  11.5 us (7%)
  local copies, waits for them, and re-layouts  2.14 us (1%)
    reduce_scatter x2, waiting for transfers between devices, summed_rows(): lax.psum_scatter(everything.astype(jnp.bfloat16), axis, scatter_dimension...  35.3 us
    ppermute x8, starting transfers between devices, passed_along(): lax.ppermute(value, axis, [(source, source + steps) for source in range(i...  33.4 us
    dot_general x8, matrix products, weighted_values(): jnp.einsum('hts,shd->thd', weights, value_block.astype(jnp.float32), prec...  13.6 us
    psum x1, blocking collectives, shards(): lax.psum((jnp.sum(convolved, axis=1), jnp.sum(convolved * convolved, axis...  13.2 us
    ppermute x8, waiting for transfers between devices, passed_along(): lax.ppermute(value, axis, [(source, source + steps) for source in range(i...  8.9 us
    another operation x8, other arithmetic, stick_terms(): inside = lax.cumsum(log_rest, axis=2, reverse=True) - log_rest  7.22 us
    all_gather x1, blocking collectives, shards(): lax.all_gather(hidden_in, 'tp', axis=0, tiled=True)  6.63 us
    psum x1, blocking collectives, shards(): squares = lax.psum(jnp.sum(merged * merged, axis=1), 'tp')  6.05 us
  transfers between devices with their start and end apart: 10, of which 9 were waited for; matrix products, arithmetic and copies ran while one was open for 19% of the time, Pallas kernels for 0%

commit v1 on v0

v1 whole, which is shorter than its diff:
```python
from functools import partial
import math

import jax
import jax.numpy as jnp
from jax import lax
from jax.experimental import pallas as pl
from jax.experimental.pallas import tpu as pltpu
from jax.sharding import PartitionSpec as P

HEAD_DIM = 128
WIDTH = 31
EPSILON = 1e-06
HALO = 32
MESH = pl.DeviceIdType.MESH


def mm(left, right):
    return jnp.dot(left, right, preferred_element_type=jnp.float32)


def row(ref):
    return ref[...].reshape(1, ref.shape[0])


def whole_layer(
    sp_count,
    tp_count,
    pair,
    hidden_in,
    pre_gain,
    w_query,
    w_key,
    w_value,
    stick_offset,
    w_glu_a,
    w_glu_b,
    w_gate_attn,
    w_gate_conv,
    conv_taps,
    conv_bias,
    norm_gain,
    norm_shift,
    w_attn_out,
    w_conv_out,
    post_gain,
    out,
    hidden_all,
    pre_gain_v,
    wq,
    wk,
    wv,
    wa,
    wb,
    wga,
    wgc,
    taps,
    bias,
    gain,
    shift,
    wo,
    wc,
    post_gain_v,
    normed,
    kv,
    gated,
    gated_f32,
    attn_out,
    attn_in,
    conv_out,
    conv_in,
    stat_out,
    stat_in,
    square_out,
    square_in,
    local_sem,
    hidden_send,
    hidden_recv,
    column_send,
    across_send,
    relay_send,
    kv_recv,
    halo_send,
    halo_recv,
    attn_send,
    attn_recv,
    conv_send,
    conv_recv,
    stat_send,
    stat_recv,
    square_send,
    square_recv,
):
    part, width = hidden_in.shape
    rows = part * tp_count
    channels = w_glu_a.shape[1]
    kv_width = w_key.shape[1]
    heads = stick_offset.shape[0]
    out_cols = post_gain.shape[0]
    outer = sp_count // pair
    sp = lax.axis_index("sp")
    tp = lax.axis_index("tp")
    z, x = sp // pair, sp % pair
    f32, bf16 = jnp.float32, jnp.bfloat16

    local_pairs = (
        (hidden_in, hidden_all.at[tp]),
        (pre_gain, pre_gain_v),
        (w_key, wk),
        (w_value, wv),
        (w_glu_a, wa),
        (w_glu_b, wb),
        (w_query, wq),
        (conv_taps, taps),
        (conv_bias, bias),
        (norm_gain, gain),
        (norm_shift, shift),
        (w_gate_attn, wga),
        (w_gate_conv, wgc),
        (w_conv_out, wc),
        (w_attn_out, wo),
        (post_gain, post_gain_v),
    )
    loads = [
        pltpu.make_async_copy(source, target, local_sem.at[index])
        for index, (source, target) in enumerate(local_pairs)
    ]
    (
        l_hidden, l_pre, l_key, l_value, l_a, l_b, l_query, l_taps, l_bias, l_gain, l_shift,
        l_ga, l_gc, l_wc, l_wo, l_post,
    ) = loads
    for load in loads:
        load.start()

    barrier = pltpu.get_barrier_semaphore()

    def greet(sp_index, tp_index):
        pl.semaphore_signal(barrier, inc=1, device_id=(sp_index, tp_index), device_id_type=MESH)

    for step in range(1, tp_count):
        greet(sp, lax.rem(tp + step, tp_count))
    for step in range(1, outer):
        greet(lax.rem(z + step, outer) * pair + x, tp)
    if pair == 2:
        greet(z * pair + (1 - x), tp)
    greetings = tp_count - 1 + outer - 1 + (pair - 1)
    if pair == 2:
        with_next = (x == 1) & (z < outer - 1)
        with_previous = (x == 0) & (z > 0)

        @pl.when(with_next)
        def _():
            greet(sp + 1, tp)

        @pl.when(with_previous)
        def _():
            greet(sp - 1, tp)

        greetings = greetings + jnp.where(with_next | with_previous, 1, 0)

    pl.semaphore_wait(barrier, greetings)

    def remote(source, target, send_sem, recv_sem, sp_index, tp_index):
        return pltpu.make_async_remote_copy(
            src_ref=source,
            dst_ref=target,
            send_sem=send_sem,
            recv_sem=recv_sem,
            device_id=(sp_index, tp_index),
            device_id_type=MESH,
        )

    peers = [lax.rem(tp + step, tp_count) for step in range(1, tp_count)]

    def exchange(source, target, send_sem, recv_sem, peer, varied):
        piece = source.at[peer] if varied else source
        return remote(piece, target.at[tp], send_sem.at[peer], recv_sem.at[tp], sp, peer)

    def arrival(target, send_sem, recv_sem, peer):
        return remote(
            target.at[peer], target.at[peer], send_sem.at[peer], recv_sem.at[peer], sp, peer
        )

    l_hidden.wait()
    hidden_copies = [
        exchange(hidden_all.at[tp], hidden_all, hidden_send, hidden_recv, peer, False)
        for peer in peers
    ]
    for copy in hidden_copies:
        copy.start()
    l_pre.wait()
    for peer in peers:
        arrival(hidden_all, hidden_send, hidden_recv, peer).wait_recv()
    for index in range(tp_count):
        values = hidden_all[index].astype(f32)
        inverse = lax.rsqrt(jnp.mean(values * values, axis=1, keepdims=True) + EPSILON)
        normed[index * part : (index + 1) * part, :] = (
            values * inverse * row(pre_gain_v)
        ).astype(bf16)

    def project(weight):
        return mm(normed[...], weight[...]).astype(bf16)

    l_key.wait()
    kv[sp, :, :kv_width] = project(wk)
    l_value.wait()
    kv[sp, :, kv_width:] = project(wv)

    def column_copy(target_z):
        return remote(
            kv.at[sp], kv.at[sp], column_send.at[target_z], kv_recv.at[sp],
            target_z * pair + x, tp,
        )

    def across_copy():
        return remote(kv.at[sp], kv.at[sp], across_send, kv_recv.at[sp], sp + 1, tp)

    def relay_copy(source_z):
        block = source_z * pair + x
        return remote(
            kv.at[block], kv.at[block], relay_send.at[source_z], kv_recv.at[block],
            z * pair + (1 - x), tp,
        )

    def block_arrival(block):
        return remote(
            kv.at[block], kv.at[block], across_send, kv_recv.at[block], sp, lax.rem(tp + 1, tp_count)
        )

    if pair == 2:

        @pl.when(x == 0)
        def _():
            across_copy().start()
            kv[sp + 1] = jnp.zeros(kv.shape[1:], bf16)

    @pl.loop(z + 1, outer)
    def _(target_z):
        column_copy(target_z).start()

    def relay(source_z):
        block_arrival(source_z * pair + x).wait_recv()
        if pair == 2:
            relay_copy(source_z).start()

    l_a.wait()
    left = project(wa).astype(f32)
    l_b.wait()
    right = project(wb).astype(f32)
    gated[HALO:, :] = (left * jax.nn.sigmoid(right)).astype(bf16)

    def halo_copy():
        return remote(
            gated.at[pl.ds(rows, HALO)], gated.at[pl.ds(0, HALO)], halo_send, halo_recv,
            jnp.minimum(sp + 1, sp_count - 1) if pair == 1 else sp + 1, tp,
        )

    @pl.when(sp < sp_count - 1)
    def _():
        halo_copy().start()

    @pl.when(sp == 0)
    def _():
        gated[:HALO, :] = jnp.zeros((HALO, channels), bf16)

    l_query.wait()
    queries = project(wq)

    early = min(outer - 1, 3)

    def early_relay(step):
        if step <= early:

            @pl.when(z >= step)
            def _():
                relay(z - step)

    early_relay(1)
    l_ga.wait()
    gate_attn = jax.nn.sigmoid(project(wga).astype(f32))
    early_relay(2)
    l_gc.wait()
    gate_conv = jax.nn.sigmoid(project(wgc).astype(f32))
    early_relay(3)

    @pl.when(sp > 0)
    def _():
        halo_copy().wait_recv()

    for load in (l_taps, l_bias, l_gain, l_shift):
        load.wait()
    gated_f32[...] = gated[...].astype(f32)
    sums = [jnp.broadcast_to(row(bias), (rows, channels))] + [jnp.zeros((rows, channels), f32)] * 3
    for tap in range(WIDTH):
        first = HALO - (WIDTH - 1) + tap
        sums[tap % 4] = sums[tap % 4] + taps[tap : tap + 1, :] * gated_f32[first : first + rows, :]
    convolved = (sums[0] + sums[1]) + (sums[2] + sums[3])

    def turned(columns):
        lane = lax.broadcasted_iota(jnp.int32, (rows, 128), 1)
        tile = jnp.zeros((rows, 128), f32)
        for index, column in enumerate(columns):
            tile = jnp.where(lane == index, column, tile)
        return jnp.transpose(tile)[:8, :]

    def turned_back(tile):
        full = jnp.concatenate([tile, jnp.zeros((120, rows), f32)], axis=0)
        return jnp.transpose(full)

    stat_out[...] = turned(
        [
            jnp.sum(convolved, axis=1, keepdims=True),
            jnp.sum(convolved * convolved, axis=1, keepdims=True),
        ]
    )
    for peer in peers:
        exchange(stat_out, stat_in, stat_send, stat_recv, peer, False).start()

    stacked = heads * rows
    scale = 1.0 / math.sqrt(HEAD_DIM)
    keys_step = pair * rows
    offset_column = jnp.concatenate(
        [jnp.full((rows, 1), stick_offset[head], f32) for head in range(heads)], axis=0
    )
    later = (
        lax.broadcasted_iota(jnp.int32, (keys_step, keys_step), 0)
        > lax.broadcasted_iota(jnp.int32, (keys_step, keys_step), 1)
    ).astype(bf16)

    def attend(pair_index, state, causal):
        total, summed = state
        blocks = kv[pl.ds(pair_index * pair, pair)].reshape(keys_step, 2 * kv_width)
        scores = jnp.concatenate(
            [
                lax.dot_general(
                    queries[:, head * HEAD_DIM : (head + 1) * HEAD_DIM],
                    blocks[:, head * HEAD_DIM : (head + 1) * HEAD_DIM],
                    (((1,), (1,)), ((), ())),
                    preferred_element_type=f32,
                )
                for head in range(heads)
            ],
            axis=0,
        )
        scores = scores * scale + offset_column
        small = jnp.log(1.0 + jnp.exp(-jnp.abs(scores)))
        rest = -(jnp.maximum(scores, 0.0) + small)
        if causal is not None:
            rest = jnp.where(causal, rest, 0.0)
        high = rest.astype(bf16)
        low = (rest - high.astype(f32)).astype(bf16)
        inside = mm(high, later) + mm(low, later)
        weights = jnp.exp(jnp.minimum(scores, 0.0) - small + inside + total)
        if causal is not None:
            weights = jnp.where(causal, weights, 0.0)
        weights = weights.astype(bf16)
        added = jnp.concatenate(
            [
                mm(
                    weights[head * rows : (head + 1) * rows],
                    blocks[:, kv_width + head * HEAD_DIM : kv_width + (head + 1) * HEAD_DIM],
                )
                for head in range(heads)
            ],
            axis=0,
        )
        return (total + jnp.sum(rest, axis=1, keepdims=True), summed + added)

    if pair == 2:

        @pl.when(x == 1)
        def _():
            block_arrival(sp - 1).wait_recv()

    token = lax.broadcasted_iota(jnp.int32, (rows, keys_step), 0)
    token = jnp.concatenate([token] * heads, axis=0) + x * rows
    causal = lax.broadcasted_iota(jnp.int32, (stacked, keys_step), 1) < token
    state = attend(
        z, (jnp.zeros((stacked, 1), f32), jnp.zeros((stacked, HEAD_DIM), f32)), causal
    )

    stats = stat_out[...]
    for peer in peers:
        arrival(stat_in, stat_send, stat_recv, peer).wait_recv()
        stats = stats + stat_in[peer]
    stats = turned_back(stats) / (channels * tp_count)
    mean = stats[:, 0:1]
    spread = stats[:, 1:2] - mean * mean
    conv_normed = jax.nn.silu(
        (convolved - mean) * lax.rsqrt(spread + EPSILON) * row(gain) + row(shift)
    ).astype(bf16)

    def branch(values, weight, sent, received, send_sem, recv_sem):
        def term(peer):
            return mm(values, weight[:, pl.ds(pl.multiple_of(peer * out_cols, 128), out_cols)])

        for peer in peers:
            sent[peer] = term(peer).astype(bf16)
            exchange(sent, received, send_sem, recv_sem, peer, True).start()
        return term(tp)

    def branch_sum(own, received, send_sem, recv_sem):
        for peer in peers:
            arrival(received, send_sem, recv_sem, peer).wait_recv()
            own = own + received[peer].astype(f32)
        return own.astype(bf16).astype(f32)

    l_wc.wait()
    conv_own = branch(conv_normed, wc, conv_out, conv_in, conv_send, conv_recv)

    def earlier(step, state):
        source_z = z - step
        if outer - 1 > early:

            @pl.when(step > early)
            def _():
                relay(source_z)

        if pair == 2:
            block_arrival(source_z * pair + (1 - x)).wait_recv()
        return attend(source_z, state, None)

    _, summed = lax.fori_loop(1, z + 1, earlier, state)
    attended = jnp.concatenate(
        [summed[head * rows : (head + 1) * rows] for head in range(heads)], axis=1
    ).astype(bf16)

    l_wo.wait()
    attn_own = branch(attended, wo, attn_out, attn_in, attn_send, attn_recv)
    merged = gate_conv * branch_sum(conv_own, conv_in, conv_send, conv_recv)
    merged = gate_attn * branch_sum(attn_own, attn_in, attn_send, attn_recv) + merged

    square_out[...] = turned([jnp.sum(merged * merged, axis=1, keepdims=True)])
    for peer in peers:
        exchange(square_out, square_in, square_send, square_recv, peer, False).start()
    l_post.wait()
    scaled = merged * row(post_gain_v)
    squares = square_out[...]
    for peer in peers:
        arrival(square_in, square_send, square_recv, peer).wait_recv()
        squares = squares + square_in[peer]
    squares = turned_back(squares)[:, 0:1]
    out[...] = (scaled * lax.rsqrt(squares / width + EPSILON)).astype(bf16)

    for peer in peers:
        exchange(hidden_all.at[tp], hidden_all, hidden_send, hidden_recv, peer, False).wait_send()
        exchange(stat_out, stat_in, stat_send, stat_recv, peer, False).wait_send()
        exchange(conv_out, conv_in, conv_send, conv_recv, peer, True).wait_send()
        exchange(attn_out, attn_in, attn_send, attn_recv, peer, True).wait_send()
        exchange(square_out, square_in, square_send, square_recv, peer, False).wait_send()
    if pair == 2:

        @pl.when(x == 0)
        def _():
            across_copy().wait_send()

    @pl.loop(z + 1, outer)
    def _(target_z):
        column_copy(target_z).wait_send()

    if pair == 2:

        @pl.loop(0, z)
        def _(source_z):
            relay_copy(source_z).wait_send()

    @pl.when(sp < sp_count - 1)
    def _():
        halo_copy().wait_send()


def shards(sp_count, tp_count, *arguments):
    (
        hidden_in, pre_gain, w_query, w_key, w_value, stick_offset, w_glu_a, w_glu_b,
        w_gate_attn, w_gate_conv, conv_taps, conv_bias, norm_gain, norm_shift,
        w_attn_out, w_conv_out, post_gain,
    ) = arguments
    pair = 2 if sp_count % 2 == 0 else 1
    part, width = hidden_in.shape
    rows = part * tp_count
    channels = w_glu_a.shape[1]
    kv_width = w_key.shape[1]
    out_cols = post_gain.shape[0]
    outer = sp_count // pair
    f32, bf16 = jnp.float32, jnp.bfloat16
    dma = pltpu.SemaphoreType.DMA

    def like(array):
        return pltpu.VMEM(array.shape, array.dtype)

    in_specs = [
        pl.BlockSpec(memory_space=pltpu.SMEM if index == 5 else pl.ANY)
        for index in range(len(arguments))
    ]
    branch_shape = (tp_count, rows, out_cols)
    return pl.pallas_call(
        partial(whole_layer, sp_count, tp_count, pair),
        out_shape=jax.ShapeDtypeStruct((rows, out_cols), bf16),
        in_specs=in_specs,
        out_specs=pl.BlockSpec(memory_space=pltpu.VMEM),
        scratch_shapes=[
            pltpu.VMEM((tp_count, part, width), bf16),
            like(pre_gain),
            like(w_query),
            like(w_key),
            like(w_value),
            like(w_glu_a),
            like(w_glu_b),
            like(w_gate_attn),
            like(w_gate_conv),
            like(conv_taps),
            like(conv_bias),
            like(norm_gain),
            like(norm_shift),
            like(w_attn_out),
            like(w_conv_out),
            like(post_gain),
            pltpu.VMEM((rows, width), bf16),
            pltpu.VMEM((sp_count, rows, 2 * kv_width), bf16),
            pltpu.VMEM((HALO + rows, channels), bf16),
            pltpu.VMEM((HALO + rows, channels), f32),
            pltpu.VMEM(branch_shape, bf16),
            pltpu.VMEM(branch_shape, bf16),
            pltpu.VMEM(branch_shape, bf16),
            pltpu.VMEM(branch_shape, bf16),
            pltpu.VMEM((8, rows), f32),
            pltpu.VMEM((tp_count, 8, rows), f32),
            pltpu.VMEM((8, rows), f32),
            pltpu.VMEM((tp_count, 8, rows), f32),
            dma((16,)),
            dma((tp_count,)),
            dma((tp_count,)),
            dma((outer,)),
            dma,
            dma((outer,)),
            dma((sp_count,)),
            dma,
            dma,
            dma((tp_count,)),
            dma((tp_count,)),
            dma((tp_count,)),
            dma((tp_count,)),
            dma((tp_count,)),
            dma((tp_count,)),
            dma((tp_count,)),
            dma((tp_count,)),
        ],
        compiler_params=pltpu.CompilerParams(
            collective_id=0, has_side_effects=True, vmem_limit_bytes=60 * 1024 * 1024
        ),
    )(*arguments)


def solution(mesh):
    in_specs = (
        P(("sp", "tp"), None),
        P(),
        P(None, "tp"),
        P(None, "tp"),
        P(None, "tp"),
        P("tp"),
        P(None, "tp"),
        P(None, "tp"),
        P(None, "tp"),
        P(None, "tp"),
        P(None, "tp"),
        P("tp"),
        P("tp"),
        P("tp"),
        P("tp", None),
        P("tp", None),
        P("tp"),
    )
    body = partial(shards, mesh.shape["sp"], mesh.shape["tp"])
    return jax.shard_map(
        body, mesh=mesh, in_specs=in_specs, out_specs=P("sp", "tp"), check_vma=False
    )
```

time: 158 us -> 33.7 us (0.21)
  the two profiles are of different devices: /device:TPU:19 before, /device:TPU:17 now
where the time goes in v1:
time: 33.7 us; the launch traced here: 33.5 us
  Pallas kernels  32 us (95%)
  local copies, waits for them, and re-layouts  1.47 us (4%)
    pallas_call x1, Pallas kernels, shards(): pl.pallas_call(partial(whole_layer, sp_count, tp_count, pair), out_shape=...  32 us
    unnamed x1, local copies, waits for them, and re-layouts  1.47 us

profile of v1, /device:TPU:17, one launch (start us, length us, event | category | flops | bytes accessed | tf_op | source)
XLA Modules:
  0.0 33.5 jit_solution(15263374028241752944)
XLA Ops:
  0.0 32.0 %shard_map.163 = bf16[64,512]{1,0:T(8,128)(2,1)} custom-call(bf16[16,2048]{1,0:T(8,128)(2,1)} %hidden_in.1, f32[2048]{0:T(1024)} %pre_gain.1, bf16[2048,256]{1,0:T(8,128)(2,1)} %w_query.1, bf16[2048,256]{1,0:T(8,128)(2,1)} %w_key.1, bf16[2048,256]{1,0:T(8,128)(2,1)} %w_value.1, f32[2]{0:T(128)} %stick_offset.1, bf16[2048,256]{1,0:T(8,128)(2,1)} %w_glu_a.1, ...), custom_call_target="tpu_custom_call" | custom-call | tf_op jit(solution)/shard_map/pallas_call | solution.py:496
  32.0 1.5 %copy.19 = bf16[64,512]{1,0:T(8,128)(2,1)} copy(bf16[64,512]{1,0:T(8,128)(2,1)} %shard_map.163) | data formatting | bytes 131072

commit v2 on v1

--- a/solution.py
+++ b/solution.py
@@ -74,6 +74,7 @@
     square_out,
     square_in,
     local_sem,
+    ready,
     hidden_send,
     hidden_recv,
     column_send,
@@ -98,6 +99,8 @@
     heads = stick_offset.shape[0]
     out_cols = post_gain.shape[0]
     outer = sp_count // pair
+    size = 2 if tp_count % 2 == 0 else 1
+    groups = tp_count // size
     sp = lax.axis_index("sp")
     tp = lax.axis_index("tp")
     z, x = sp // pair, sp % pair
@@ -139,26 +142,19 @@
 
     for step in range(1, tp_count):
         greet(sp, lax.rem(tp + step, tp_count))
-    for step in range(1, outer):
-        greet(lax.rem(z + step, outer) * pair + x, tp)
     if pair == 2:
         greet(z * pair + (1 - x), tp)
-    greetings = tp_count - 1 + outer - 1 + (pair - 1)
-    if pair == 2:
-        with_next = (x == 1) & (z < outer - 1)
-        with_previous = (x == 0) & (z > 0)
-
-        @pl.when(with_next)
-        def _():
-            greet(sp + 1, tp)
-
-        @pl.when(with_previous)
-        def _():
-            greet(sp - 1, tp)
-
-        greetings = greetings + jnp.where(with_next | with_previous, 1, 0)
-
-    pl.semaphore_wait(barrier, greetings)
+
+    @pl.when(z > 0)
+    def _():
+        greet(sp - pair, tp)
+
+    @pl.when(z < outer - 1)
+    def _():
+        greet(sp + pair, tp)
+
+    beside = jnp.where(z > 0, 1, 0) + jnp.where(z < outer - 1, 1, 0)
+    pl.semaphore_wait(barrier, tp_count - 1 + (pair - 1) + beside)
 
     def remote(source, target, send_sem, recv_sem, sp_index, tp_index):
         return pltpu.make_async_remote_copy(
@@ -188,60 +184,97 @@
     ]
     for copy in hidden_copies:
         copy.start()
+
+    @pl.when(z < outer - 1)
+    def _():
+        pl.semaphore_wait(ready, 1)
+
+    @pl.when(z > 0)
+    def _():
+        pl.semaphore_signal(ready, inc=1, device_id=(sp - pair, tp), device_id_type=MESH)
+
     l_pre.wait()
-    for peer in peers:
-        arrival(hidden_all, hidden_send, hidden_recv, peer).wait_recv()
-    for index in range(tp_count):
-        values = hidden_all[index].astype(f32)
-        inverse = lax.rsqrt(jnp.mean(values * values, axis=1, keepdims=True) + EPSILON)
-        normed[index * part : (index + 1) * part, :] = (
-            values * inverse * row(pre_gain_v)
-        ).astype(bf16)
 
     def project(weight):
         return mm(normed[...], weight[...]).astype(bf16)
 
-    l_key.wait()
-    kv[sp, :, :kv_width] = project(wk)
-    l_value.wait()
-    kv[sp, :, kv_width:] = project(wv)
-
-    def column_copy(target_z):
+    def group_rows(group):
+        first = lax.rem(tp // size + group, groups) * (size * part)
+        return pl.ds(pl.multiple_of(first, size * part), size * part)
+
+    def kv_copy(block, group, send_sem, sp_index):
+        piece = kv.at[block, group_rows(group)]
+        return remote(piece, piece, send_sem, kv_recv.at[block, group], sp_index, tp)
+
+    def column_copy(target_z, group):
+        return kv_copy(sp, group, column_send.at[target_z, group], target_z * pair + x)
+
+    def across_copy(group):
+        return kv_copy(sp, group, across_send.at[group], sp + 1)
+
+    def relay_copy(source_z, group):
+        return kv_copy(
+            source_z * pair + x, group, relay_send.at[source_z, group], z * pair + (1 - x)
+        )
+
+    def block_arrival(block, group):
+        piece = kv.at[block, group_rows(group)]
         return remote(
-            kv.at[sp], kv.at[sp], column_send.at[target_z], kv_recv.at[sp],
-            target_z * pair + x, tp,
+            piece, piece, across_send.at[group], kv_recv.at[block, group], sp,
+            lax.rem(tp + 1, tp_count),
         )
 
-    def across_copy():
-        return remote(kv.at[sp], kv.at[sp], across_send, kv_recv.at[sp], sp + 1, tp)
-
-    def relay_copy(source_z):
-        block = source_z * pair + x
-        return remote(
-            kv.at[block], kv.at[block], relay_send.at[source_z], kv_recv.at[block],
-            z * pair + (1 - x), tp,
-        )
-
-    def block_arrival(block):
-        return remote(
-            kv.at[block], kv.at[block], across_send, kv_recv.at[block], sp, lax.rem(tp + 1, tp_count)
-        )
+    def relay(source_z, group):
+        block_arrival(source_z * pair + x, group).wait_recv()
+        if pair == 2:
+            relay_copy(source_z, group).start()
+
+    for group in range(groups):
+        for member in range(size):
+            index = lax.rem(tp // size + group, groups) * size + member
+            if group == 0:
+
+                @pl.when(index != tp)
+                def _():
+                    arrival(hidden_all, hidden_send, hidden_recv, index).wait_recv()
+
+            else:
+                arrival(hidden_all, hidden_send, hidden_recv, index).wait_recv()
+            values = hidden_all[index].astype(f32)
+            inverse = lax.rsqrt(jnp.mean(values * values, axis=1, keepdims=True) + EPSILON)
+            normed[pl.ds(pl.multiple_of(index * part, part), part), :] = (
+                values * inverse * row(pre_gain_v)
+            ).astype(bf16)
+        if group == 0:
+            l_key.wait()
+            l_value.wait()
+        tokens = normed[group_rows(group), :]
+        kv[sp, group_rows(group), :kv_width] = mm(tokens, wk[...]).astype(bf16)
+        kv[sp, group_rows(group), kv_width:] = mm(tokens, wv[...]).astype(bf16)
+        if pair == 2:
+
+            @pl.when(x == 0)
+            def _():
+                across_copy(group).start()
+
+        @pl.loop(z + 1, outer)
+        def _(target_z):
+            column_copy(target_z, group).start()
 
     if pair == 2:
 
         @pl.when(x == 0)
         def _():
-            across_copy().start()
             kv[sp + 1] = jnp.zeros(kv.shape[1:], bf16)
 
-    @pl.loop(z + 1, outer)
-    def _(target_z):
-        column_copy(target_z).start()
-
-    def relay(source_z):
-        block_arrival(source_z * pair + x).wait_recv()
-        if pair == 2:
-            relay_copy(source_z).start()
+    def early_relay(group, step):
+        if step <= early and group < groups:
+
+            @pl.when(z >= step)
+            def _():
+                relay(z - step, group)
+
+    early = min(outer - 1, 3)
 
     l_a.wait()
     left = project(wa).astype(f32)
@@ -263,25 +296,17 @@
     def _():
         gated[:HALO, :] = jnp.zeros((HALO, channels), bf16)
 
+    early_relay(0, 1)
     l_query.wait()
     queries = project(wq)
 
-    early = min(outer - 1, 3)
-
-    def early_relay(step):
-        if step <= early:
-
-            @pl.when(z >= step)
-            def _():
-                relay(z - step)
-
-    early_relay(1)
+    early_relay(0, 2)
     l_ga.wait()
     gate_attn = jax.nn.sigmoid(project(wga).astype(f32))
-    early_relay(2)
+    early_relay(0, 3)
     l_gc.wait()
     gate_conv = jax.nn.sigmoid(project(wgc).astype(f32))
-    early_relay(3)
+    early_relay(1, 1)
 
     @pl.when(sp > 0)
     def _():
@@ -370,7 +395,8 @@
 
         @pl.when(x == 1)
         def _():
-            block_arrival(sp - 1).wait_recv()
+            for group in range(groups):
+                block_arrival(sp - 1, group).wait_recv()
 
     token = lax.broadcasted_iota(jnp.int32, (rows, keys_step), 0)
     token = jnp.concatenate([token] * heads, axis=0) + x * rows
@@ -408,16 +434,24 @@
     l_wc.wait()
     conv_own = branch(conv_normed, wc, conv_out, conv_in, conv_send, conv_recv)
 
+    @pl.loop(early + 1, z + 1)
+    def _(step):
+        relay(z - step, 0)
+
     def earlier(step, state):
         source_z = z - step
-        if outer - 1 > early:
-
-            @pl.when(step > early)
-            def _():
-                relay(source_z)
+        for group in range(1, groups):
+            if group > 1:
+                relay(source_z, group)
+            else:
+
+                @pl.when(step < z)
+                def _():
+                    relay(source_z - 1, group)
 
         if pair == 2:
-            block_arrival(source_z * pair + (1 - x)).wait_recv()
+            for group in range(groups):
+                block_arrival(source_z * pair + (1 - x), group).wait_recv()
         return attend(source_z, state, None)
 
     _, summed = lax.fori_loop(1, z + 1, earlier, state)
@@ -448,21 +482,20 @@
         exchange(conv_out, conv_in, conv_send, conv_recv, peer, True).wait_send()
         exchange(attn_out, attn_in, attn_send, attn_recv, peer, True).wait_send()
         exchange(square_out, square_in, square_send, square_recv, peer, False).wait_send()
-    if pair == 2:
-
-        @pl.when(x == 0)
-        def _():
-            across_copy().wait_send()
-
-    @pl.loop(z + 1, outer)
-    def _(target_z):
-        column_copy(target_z).wait_send()
-
-    if pair == 2:
-
-        @pl.loop(0, z)
-        def _(source_z):
-            relay_copy(source_z).wait_send()
+    for group in range(groups):
+        if pair == 2:
+
+            @pl.when(x == 0)
+            def _():
+                across_copy(group).wait_send()
+
+            @pl.loop(0, z)
+            def _(source_z):
+                relay_copy(source_z, group).wait_send()
+
+        @pl.loop(z + 1, outer)
+        def _(target_z):
+            column_copy(target_z, group).wait_send()
 
     @pl.when(sp < sp_count - 1)
     def _():
@@ -482,6 +515,7 @@
     kv_width = w_key.shape[1]
     out_cols = post_gain.shape[0]
     outer = sp_count // pair
+    groups = tp_count // (2 if tp_count % 2 == 0 else 1)
     f32, bf16 = jnp.float32, jnp.bfloat16
     dma = pltpu.SemaphoreType.DMA
 
@@ -528,12 +562,13 @@
             pltpu.VMEM((8, rows), f32),
             pltpu.VMEM((tp_count, 8, rows), f32),
             dma((16,)),
-            dma((tp_count,)),
-            dma((tp_count,)),
-            dma((outer,)),
-            dma,
-            dma((outer,)),
-            dma((sp_count,)),
+            pltpu.SemaphoreType.REGULAR,
+            dma((tp_count,)),
+            dma((tp_count,)),
+            dma((outer, groups)),
+            dma((groups,)),
+            dma((outer, groups)),
+            dma((sp_count, groups)),
             dma,
             dma,
             dma((tp_count,)),

time: 33.7 us -> 31.7 us (0.941)
  the two profiles are of different devices: /device:TPU:17 before, /device:TPU:27 now
where the time goes in v2:
time: 31.7 us; the launch traced here: 31.6 us
  Pallas kernels  30.1 us (95%)
  local copies, waits for them, and re-layouts  1.47 us (5%)
    pallas_call x1, Pallas kernels, shards(): pl.pallas_call(partial(whole_layer, sp_count, tp_count, pair), out_shape=...  30.1 us
    unnamed x1, local copies, waits for them, and re-layouts  1.47 us

profile of v2, /device:TPU:27, one launch (start us, length us, event | category | flops | bytes accessed | tf_op | source)
XLA Modules:
  0.0 31.6 jit_solution(1332845242166125728)
XLA Ops:
  0.0 30.1 %shard_map.163 = bf16[64,512]{1,0:T(8,128)(2,1)} custom-call(bf16[16,2048]{1,0:T(8,128)(2,1)} %hidden_in.1, f32[2048]{0:T(1024)} %pre_gain.1, bf16[2048,256]{1,0:T(8,128)(2,1)} %w_query.1, bf16[2048,256]{1,0:T(8,128)(2,1)} %w_key.1, bf16[2048,256]{1,0:T(8,128)(2,1)} %w_value.1, f32[2]{0:T(128)} %stick_offset.1, bf16[2048,256]{1,0:T(8,128)(2,1)} %w_glu_a.1, ...), custom_call_target="tpu_custom_call" | custom-call | tf_op jit(solution)/shard_map/pallas_call | solution.py:530
  30.1 1.5 %copy.19 = bf16[64,512]{1,0:T(8,128)(2,1)} copy(bf16[64,512]{1,0:T(8,128)(2,1)} %shard_map.163) | data formatting | bytes 131072

commit v3 on v2

--- a/solution.py
+++ b/solution.py
@@ -166,7 +166,12 @@
             device_id_type=MESH,
         )
 
-    peers = [lax.rem(tp + step, tp_count) for step in range(1, tp_count)]
+    peers = [
+        lax.rem(tp // size + group, groups) * size + lax.rem(tp + member, size)
+        for group in [*range(1, groups), 0]
+        for member in range(1 if group == 0 else 0, size)
+    ]
+    senders = peers[::-1]
 
     def exchange(source, target, send_sem, recv_sem, peer, varied):
         piece = source.at[peer] if varied else source
@@ -258,8 +263,8 @@
                 across_copy(group).start()
 
         @pl.loop(z + 1, outer)
-        def _(target_z):
-            column_copy(target_z, group).start()
+        def _(turn):
+            column_copy(outer + z - turn, group).start()
 
     if pair == 2:
 
@@ -300,13 +305,9 @@
     l_query.wait()
     queries = project(wq)
 
-    early_relay(0, 2)
     l_ga.wait()
     gate_attn = jax.nn.sigmoid(project(wga).astype(f32))
-    early_relay(0, 3)
-    l_gc.wait()
-    gate_conv = jax.nn.sigmoid(project(wgc).astype(f32))
-    early_relay(1, 1)
+    early_relay(0, 2)
 
     @pl.when(sp > 0)
     def _():
@@ -340,6 +341,11 @@
     )
     for peer in peers:
         exchange(stat_out, stat_in, stat_send, stat_recv, peer, False).start()
+
+    early_relay(0, 3)
+    l_gc.wait()
+    gate_conv = jax.nn.sigmoid(project(wgc).astype(f32))
+    early_relay(1, 1)
 
     stacked = heads * rows
     scale = 1.0 / math.sqrt(HEAD_DIM)
@@ -406,7 +412,7 @@
     )
 
     stats = stat_out[...]
-    for peer in peers:
+    for peer in senders:
         arrival(stat_in, stat_send, stat_recv, peer).wait_recv()
         stats = stats + stat_in[peer]
     stats = turned_back(stats) / (channels * tp_count)
@@ -426,7 +432,7 @@
         return term(tp)
 
     def branch_sum(own, received, send_sem, recv_sem):
-        for peer in peers:
+        for peer in senders:
             arrival(received, send_sem, recv_sem, peer).wait_recv()
             own = own + received[peer].astype(f32)
         return own.astype(bf16).astype(f32)
@@ -470,7 +476,7 @@
     l_post.wait()
     scaled = merged * row(post_gain_v)
     squares = square_out[...]
-    for peer in peers:
+    for peer in senders:
         arrival(square_in, square_send, square_recv, peer).wait_recv()
         squares = squares + square_in[peer]
     squares = turned_back(squares)[:, 0:1]

time: 31.7 us -> 30.8 us (0.972)
  the two profiles are of different devices: /device:TPU:27 before, /device:TPU:19 now
where the time goes in v3:
time: 30.8 us; the launch traced here: 30.6 us
  Pallas kernels  29.1 us (94%)
  local copies, waits for them, and re-layouts  1.47 us (5%)
    pallas_call x1, Pallas kernels, shards(): pl.pallas_call(partial(whole_layer, sp_count, tp_count, pair), out_shape=...  29.1 us
    unnamed x1, local copies, waits for them, and re-layouts  1.47 us

profile of v3, /device:TPU:19, one launch (start us, length us, event | category | flops | bytes accessed | tf_op | source)
XLA Modules:
  0.0 30.6 jit_solution(6794827276162397041)
XLA Ops:
  0.0 29.1 %shard_map.163 = bf16[64,512]{1,0:T(8,128)(2,1)} custom-call(bf16[16,2048]{1,0:T(8,128)(2,1)} %hidden_in.1, f32[2048]{0:T(1024)} %pre_gain.1, bf16[2048,256]{1,0:T(8,128)(2,1)} %w_query.1, bf16[2048,256]{1,0:T(8,128)(2,1)} %w_key.1, bf16[2048,256]{1,0:T(8,128)(2,1)} %w_value.1, f32[2]{0:T(128)} %stick_offset.1, bf16[2048,256]{1,0:T(8,128)(2,1)} %w_glu_a.1, ...), custom_call_target="tpu_custom_call" | custom-call | tf_op jit(solution)/shard_map/pallas_call | solution.py:536
  29.1 1.5 %copy.19 = bf16[64,512]{1,0:T(8,128)(2,1)} copy(bf16[64,512]{1,0:T(8,128)(2,1)} %shard_map.163) | data formatting | bytes 131072

commit v4 on v3

--- a/solution.py
+++ b/solution.py
@@ -431,8 +431,8 @@
             exchange(sent, received, send_sem, recv_sem, peer, True).start()
         return term(tp)
 
-    def branch_sum(own, received, send_sem, recv_sem):
-        for peer in senders:
+    def branch_sum(own, received, send_sem, recv_sem, sources):
+        for peer in sources:
             arrival(received, send_sem, recv_sem, peer).wait_recv()
             own = own + received[peer].astype(f32)
         return own.astype(bf16).astype(f32)
@@ -466,9 +466,34 @@
     ).astype(bf16)
 
     l_wo.wait()
-    attn_own = branch(attended, wo, attn_out, attn_in, attn_send, attn_recv)
-    merged = gate_conv * branch_sum(conv_own, conv_in, conv_send, conv_recv)
-    merged = gate_attn * branch_sum(attn_own, attn_in, attn_send, attn_recv) + merged
+    def attn_term(peer):
+        return mm(attended, wo[:, pl.ds(pl.multiple_of(peer * out_cols, 128), out_cols)])
+
+    if size == 2:
+        sibling = tp + 1 - 2 * lax.rem(tp, 2)
+        across = [lax.rem(tp // size + group, groups) * size for group in range(1, groups)]
+        mine = [first + lax.rem(tp, 2) for first in across]
+        theirs = [first + 1 - lax.rem(tp, 2) for first in across]
+        for peer, other in zip(mine, theirs):
+            attn_out[other] = attn_term(other).astype(bf16)
+            remote(
+                attn_out.at[other], attn_in.at[peer], attn_send.at[other], attn_recv.at[peer],
+                sp, sibling,
+            ).start()
+        terms = [attn_term(peer) for peer in mine]
+        attn_out[sibling] = attn_term(sibling).astype(bf16)
+        exchange(attn_out, attn_in, attn_send, attn_recv, sibling, True).start()
+        attn_own = attn_term(tp)
+        for peer, other, term in zip(mine, theirs, terms):
+            arrival(attn_in, attn_send, attn_recv, other).wait_recv()
+            attn_out[peer] = (term + attn_in[other].astype(f32)).astype(bf16)
+            exchange(attn_out, attn_in, attn_send, attn_recv, peer, True).start()
+        attn_senders = [sibling, *mine]
+    else:
+        attn_own = branch(attended, wo, attn_out, attn_in, attn_send, attn_recv)
+        attn_senders = senders
+    merged = gate_conv * branch_sum(conv_own, conv_in, conv_send, conv_recv, senders)
+    merged = gate_attn * branch_sum(attn_own, attn_in, attn_send, attn_recv, attn_senders) + merged
 
     square_out[...] = turned([jnp.sum(merged * merged, axis=1, keepdims=True)])
     for peer in peers:

time: 30.8 us -> 31.4 us (1.019)
  Pallas kernels: 29.1 us -> 29.8 us
    pallas_call x1, Pallas kernels: 29.1 us -> 29.8 us  [shards(): pl.pallas_call(partial(whole_layer, sp_count, tp_count, pair), out_shape=...]
where the time goes in v4:
time: 31.4 us; the launch traced here: 31.2 us
  Pallas kernels  29.8 us (95%)
  local copies, waits for them, and re-layouts  1.47 us (5%)
    pallas_call x1, Pallas kernels, shards(): pl.pallas_call(partial(whole_layer, sp_count, tp_count, pair), out_shape=...  29.8 us
    unnamed x1, local copies, waits for them, and re-layouts  1.47 us

profile of v4, /device:TPU:19, one launch (start us, length us, event | category | flops | bytes accessed | tf_op | source)
XLA Modules:
  0.0 31.2 jit_solution(1497846093256626703)
XLA Ops:
  0.0 29.8 %shard_map.163 = bf16[64,512]{1,0:T(8,128)(2,1)} custom-call(bf16[16,2048]{1,0:T(8,128)(2,1)} %hidden_in.1, f32[2048]{0:T(1024)} %pre_gain.1, bf16[2048,256]{1,0:T(8,128)(2,1)} %w_query.1, bf16[2048,256]{1,0:T(8,128)(2,1)} %w_key.1, bf16[2048,256]{1,0:T(8,128)(2,1)} %w_value.1, f32[2]{0:T(128)} %stick_offset.1, bf16[2048,256]{1,0:T(8,128)(2,1)} %w_glu_a.1, ...), custom_call_target="tpu_custom_call" | custom-call | tf_op jit(solution)/shard_map/pallas_call | solution.py:561
  29.8 1.5 %copy.19 = bf16[64,512]{1,0:T(8,128)(2,1)} copy(bf16[64,512]{1,0:T(8,128)(2,1)} %shard_map.163) | data formatting | bytes 131072
